TPU v7x, 1024 devices: a whole 4x4x32 slice. The times are simulated.
1024 devices in a mesh: rep: 4 (over z_hi), fs: 32 (over z_lo, y), tp: 8 (over x, core).
Axes of the slice: x: 4, y: 4, z: 32 (z_hi: 4, z_lo: 8; z = z_hi * 8 + z_lo), core: 2. Of those that a mesh axis runs over, the one named last changes fastest.
Arguments:
- residual: bfloat16 [128, 256, 2048], P(('rep', 'fs'), None, 'tp'), may hold values from -6 to 6
- queries: bfloat16 [128, 256, 2048], P(('rep', 'fs'), None, 'tp'), may hold values from -6 to 6
- key_matrix: bfloat16 [128, 256, 2048], P(('rep', 'fs'), None, 'tp'), may hold values from -6 to 6
- value_matrix: bfloat16 [128, 256, 2048], P(('rep', 'fs'), None, 'tp'), may hold values from -6 to 6
- decay_logodds: float32 [128, 256, 2048], P(('rep', 'fs'), None, 'tp'), may hold values from -3.4 to 8.9, as said below
- decay_surge: float32 [128, 256, 8], P(('rep', 'fs'), None, 'tp'), may hold values from -2.1 to 0, as said below
- head_norm_gain: float32 [256], replicated, may hold values from 0.1 to 1.9
- output_matrix: float32 [2048, 2048], P('fs', 'tp'), may hold values from -0.125 to 0.125
- output_column_scale: float32 [2048], P('tp'), may hold values from 0.5 to 2
- premix_norm_gain: float32 [2048], replicated, may hold values from 0.1 to 1.9
- gate_matrix: float32 [2048, 2816], P('fs', 'tp'), may hold values from -0.125 to 0.125
- gate_column_scale: float32 [2816], P('tp'), may hold values from 0.5 to 2
- up_matrix: float32 [2048, 2816], P('fs', 'tp'), may hold values from -0.125 to 0.125
- up_column_scale: float32 [2816], P('tp'), may hold values from 0.5 to 2
- down_matrix: float32 [2048, 2816], P('fs', 'tp'), may hold values from -0.109375 to 0.109375
- down_column_scale: float32 [2048], P('tp'), may hold values from 0.5 to 2
Outputs:
- layer_out: bfloat16 [128, 256, 2048], P(('rep', 'fs'), None, 'tp')
Inputs may be any that keep to these rules, and one draw needn't show every extreme that they name: `decay_logodds`: log-odds of a key channel's decay. `decay_surge`: non-positive log-factors of a head's state.
All inputs are finite; a program needn't handle non-finite values.
Results may differ from a plain program's by a relative error of at most 0.018.
Values may be sent and summed in bfloat16 or wider, within the bound.
A program may use at most 32 MiB of HBM per device.

v0:
```python
import jax
import jax.numpy as jnp
from jax import lax
from jax.sharding import PartitionSpec as P

BLOCK = 64


epsilon = 1e-06
softness_factor = 16.0
highest = lax.Precision.HIGHEST


def joined_along(pieces, dim):
    pieces = jnp.moveaxis(pieces, 0, dim)
    lengths = pieces.shape
    return pieces.reshape(*lengths[:dim], lengths[dim] * lengths[dim + 1], *lengths[dim + 2 :])


def sent_to_all(x, axis):
    length = lax.axis_size(axis)
    return lax.all_to_all(jnp.broadcast_to(x[None], (length, *x.shape)), axis, 0, 0, tiled=True)


def collect(x, axis, dim):
    return joined_along(sent_to_all(x, axis), dim)


def split_up(x, dim, length):
    lengths = x.shape
    pieces = x.reshape(*lengths[:dim], length, lengths[dim] // length, *lengths[dim + 1 :])
    return jnp.moveaxis(pieces, dim, 0)


def summed_on_arrival(x, axis, dim):
    pieces = split_up(x, dim, lax.axis_size(axis))
    arrived = lax.all_to_all(pieces, axis, split_axis=0, concat_axis=0, tiled=True)
    return arrived.astype(jnp.float32).sum(axis=0)


def sent_together(arrays, axis, dim, along):
    widths = [a.shape[along] for a in arrays]
    both = jnp.concatenate(arrays, axis=along)
    whole = lax.all_gather(both, axis, axis=dim, tiled=True)
    return tuple(jnp.split(whole, [sum(widths[:k]) for k in range(1, len(widths))], axis=along))


def one_direction(query_heads, key_heads, value_heads, log_decay_values):
    sequence_batch, head_total, token_length, key_channel_width = query_heads.shape
    value_width = value_heads.shape[-1]
    block_count = token_length // BLOCK

    def blocks(tensor):
        return tensor.reshape(sequence_batch, head_total, block_count, BLOCK, tensor.shape[-1])

    q_blocks = blocks(query_heads)
    k_blocks = blocks(key_heads)
    v_blocks = blocks(value_heads)
    running = jnp.cumsum(blocks(log_decay_values), axis=3)
    block_end = running[:, :, :, -1:, :]
    q_dec = q_blocks * jnp.exp(running)
    k_inv = k_blocks * jnp.exp(-running)
    k_end = k_blocks * jnp.exp(block_end - running)
    lower_mask = jnp.tril(jnp.ones((BLOCK, BLOCK), jnp.float32))
    scores = jnp.einsum("shnid,shnjd->shnij", q_dec, k_inv, precision=highest) * lower_mask
    inner_part = jnp.einsum("shnij,shnje->shnie", scores, v_blocks, precision=highest)
    fading = jnp.exp(block_end[:, :, :, 0, :])

    def advance(memory, pieces):
        q_piece, k_piece, v_piece, f_piece = pieces
        carried = jnp.einsum("shcd,shde->shce", q_piece, memory, precision=highest)
        memory = f_piece[..., None] * memory + jnp.einsum(
            "shcd,shce->shde", k_piece, v_piece, precision=highest
        )
        return (memory, carried)

    pieces = tuple((jnp.moveaxis(tensor, 2, 0) for tensor in (q_dec, k_end, v_blocks, fading)))
    initial = jnp.zeros((sequence_batch, head_total, key_channel_width, value_width), jnp.float32)
    _, carried = lax.scan(advance, initial, pieces)
    summed = inner_part + jnp.moveaxis(carried, 0, 2)
    return summed.reshape(sequence_batch, head_total, token_length, value_width)


def backwards(tensor):
    return tensor[:, :, ::-1]


def linear_attend(queries, key_matrix, value_matrix, decay_logodds, decay_surge, head_norm_gain):
    sequence_batch, token_length, head_total = decay_surge.shape
    key_channel_width = queries.shape[-1] // head_total
    value_width = value_matrix.shape[-1] // head_total

    def split_heads(tensor, width):
        return jnp.transpose(
            tensor.astype(jnp.float32).reshape(sequence_batch, token_length, head_total, width),
            (0, 2, 1, 3),
        )

    query_heads = split_heads(queries, key_channel_width) * key_channel_width ** (-0.5)
    key_heads = split_heads(key_matrix, key_channel_width)
    value_heads = split_heads(value_matrix, value_width)
    gate_values = (
        jax.nn.log_sigmoid(decay_logodds).reshape(
            sequence_batch, token_length, head_total, key_channel_width
        )
        / softness_factor
    )
    log_decay_values = jnp.transpose(gate_values + decay_surge[..., None], (0, 2, 1, 3))
    forward = one_direction(query_heads, key_heads, value_heads, log_decay_values)
    backward = backwards(
        one_direction(
            backwards(query_heads),
            backwards(key_heads),
            backwards(value_heads),
            backwards(log_decay_values),
        )
    )
    attended = forward + backward
    scaled = (
        attended
        * lax.rsqrt(jnp.mean(attended * attended, axis=-1, keepdims=True) + epsilon)
        * head_norm_gain
    )
    merged = jnp.transpose(scaled, (0, 2, 1, 3)).reshape(
        sequence_batch * token_length, head_total * value_width
    )
    return merged.astype(jnp.bfloat16)


def by_rows(left, right):
    return lax.dot_general(
        left, right, (((1,), (1,)), ((), ())), preferred_element_type=jnp.float32
    )


def body(
    residual,
    queries,
    key_matrix,
    value_matrix,
    decay_logodds,
    decay_surge,
    head_norm_gain,
    output_matrix,
    output_column_scale,
    premix_norm_gain,
    gate_matrix,
    gate_column_scale,
    up_matrix,
    up_column_scale,
    down_matrix,
    down_column_scale,
):
    sequence_batch, token_length, local_width = residual.shape
    row_count = sequence_batch * token_length
    normalized_rows = linear_attend(
        queries, key_matrix, value_matrix, decay_logodds, decay_surge, head_norm_gain
    )
    out_half = output_matrix.astype(jnp.bfloat16)
    out_full = collect(out_half, "fs", 0)
    mix_terms = by_rows(normalized_rows, out_full)
    mix_total = summed_on_arrival(mix_terms.astype(jnp.bfloat16), "tp", 1)
    own_rows = residual.reshape(row_count, local_width).astype(jnp.float32)
    updated = (own_rows + output_column_scale * mix_total).astype(jnp.bfloat16)
    features = collect(updated, "tp", 1)
    wide_rows = features.astype(jnp.float32)
    factor = lax.rsqrt(jnp.mean(wide_rows * wide_rows, axis=-1, keepdims=True) + epsilon)
    normin = (wide_rows * factor * premix_norm_gain).astype(jnp.bfloat16)
    gate_half = gate_matrix.astype(jnp.bfloat16)
    up_half = up_matrix.astype(jnp.bfloat16)
    down_half = down_matrix.astype(jnp.bfloat16)
    gate_full, up_full, down_full = sent_together((gate_half, up_half, down_half), "fs", 0, 1)
    gate_pre = jnp.dot(normin, gate_full, preferred_element_type=jnp.float32)
    up_pre = jnp.dot(normin, up_full, preferred_element_type=jnp.float32)
    hidden = (jax.nn.silu(gate_pre * gate_column_scale) * (up_pre * up_column_scale)).astype(
        jnp.bfloat16
    )
    down_terms = by_rows(hidden, down_full)
    down_total = summed_on_arrival(down_terms.astype(jnp.bfloat16), "tp", 1)
    result = (updated.astype(jnp.float32) + down_column_scale * down_total).astype(jnp.bfloat16)
    return result.reshape(sequence_batch, token_length, local_width)


def solution(mesh):
    return jax.shard_map(
        body,
        mesh=mesh,
        in_specs=(
            P(("rep", "fs"), None, "tp"),
            P(("rep", "fs"), None, "tp"),
            P(("rep", "fs"), None, "tp"),
            P(("rep", "fs"), None, "tp"),
            P(("rep", "fs"), None, "tp"),
            P(("rep", "fs"), None, "tp"),
            P(),
            P("fs", "tp"),
            P("tp"),
            P(),
            P("fs", "tp"),
            P("tp"),
            P("fs", "tp"),
            P("tp"),
            P("fs", "tp"),
            P("tp"),
        ),
        out_specs=P(("rep", "fs"), None, "tp"),
        check_vma=False,
    )
```

profile of v0, /device:TPU:1, one launch (start us, length us, event | category | flops | bytes accessed | tf_op | source)
XLA Modules:
  0.0 303.7 jit_solution(11055281597598046256)
XLA Ops:
  6.5 0.9 convert_element_type.82
  7.4 1.1 broadcast_in_dim.21
  8.6 16.2 %all-to-all-start = ((bf16[32,64,256]{2,1,0:T(8,128)(2,1)}), bf16[32,64,256]{2,1,0:T(8,128)(2,1)S(1)}, u32[]{:S(2)}, u32[]{:S(2)}) async-start(bf16[32,64,256]{2,1,0:T(8,128)(2,1)} %broadcast_in_dim.21), calls=%async_computation | async-start | bytes 2097152 | tf_op jit(solution)/shard_map/all_to_all | solution.py:22
  24.8 0.0 all-gather.2.cloned.1.call-start
  24.9 0.8 concatenate.3
  25.7 0.0 all-gather.2.cloned.1.call-update
  25.8 0.2 reverse.11
  26.0 0.2 reverse.12
  26.2 0.2 bitcast_add_fusion
  26.4 0.1 rev.17
  26.5 0.2 reduce_window_sum.23
  26.8 1.6 reverse.10
  28.4 0.6 fusion.84
  29.0 0.8 fusion.66
  29.8 0.7 broadcast.199.clone.1
  30.6 8.8 %while.27 = (s32[]{:T(128)}, f32[1,1,256,256]{3,2,1,0:T(8,128)S(1)}, f32[4,1,1,64,256]{4,3,2,1,0:T(8,128)}, f32[4,1,1,256]{3,2,1,0:T(1,128)S(1)}, f32[4,1,1,64,2...) while((s32[]{:T(128)}, ...), condition=%wide.region_5.6_spmd.clone, body=%wide.region_4.5_spmd.clone.sunk | while | flops 100925440 | bytes 1053804 | solution.py:79
  30.6 1.7 fusion.118
  32.3 0.5 fusion.117
  32.8 1.7 fusion.118
  34.5 0.5 fusion.117
  35.0 1.7 fusion.118
  36.7 0.5 fusion.117
  37.2 1.7 fusion.118
  38.9 0.5 fusion.117
  39.4 0.0 copy-start.5
  39.4 1.3 convolution_multiply_fusion
  40.7 1.3 convolution_add_fusion
  42.0 0.1 rev.19
  42.2 0.5 broadcast.232
  42.7 0.6 reduce.6
  43.3 0.1 add.94
  43.4 0.2 fusion.57
  43.5 0.1 broadcast_add_fusion
  43.7 0.2 reduce_window_sum.21
  44.0 0.4 convolution_multiply_fusion.1
  44.4 0.1 fusion.71
  44.6 3.1 %while.26 = (s32[]{:T(128)}, f32[1,1,256,256]{3,2,1,0:T(8,128)S(1)}, f32[4,1,1,64,256]{4,3,2,1,0:T(8,128)S(1)}, f32[4,1,1,256]{3,2,1,0:T(1,128)S(1)}, f32[4,1,1,...) while((s32[]{:T(128)}, ...), condition=%wide.region_2.3_spmd.clone, body=%wide.region_1.2_spmd.clone.sunk | while | flops 100925440 | bytes 1053804 | solution.py:79
  44.6 0.3 fusion.112
  44.9 0.5 fusion.111
  45.4 0.3 fusion.112
  45.6 0.5 fusion.111
  46.1 0.3 fusion.112
  46.4 0.5 fusion.111
  46.9 0.3 fusion.112
  47.2 0.5 fusion.111
  47.7 0.2 convolution_add_fusion.1
  48.0 0.1 multiply_reduce_fusion.1
  48.1 27.0 %all-to-all-done = bf16[32,64,256]{2,1,0:T(8,128)(2,1)S(1)} async-done(((bf16[32,64,256]{2,1,0:T(8,128)(2,1)}), bf16[32,64,256]{2,1,0:T(8,128)(2,1)S(1)}, u32[]{:S(2)}, u32[]{:S(2)}) %all-to-all-start) | async-done | bytes 1048608 | tf_op jit(solution)/shard_map/all_to_all | solution.py:22
  75.1 0.5 convolution_convert_fusion.1
  75.6 0.1 copy.48
  75.7 25.7 %all_to_all.20 = bf16[8,256,256]{2,1,0:T(8,128)(2,1)S(1)} all-to-all(bf16[8,256,256]{2,1,0:T(8,128)(2,1)S(1)} %bitcast.200), channel_id=1, replica_groups=mesh['rep'=4,'fs'=32,'tp'=8] {'tp'}, dimensions={0} | all-to-all | bytes 2097152 | tf_op jit(solution)/shard_map/all_to_all | solution.py:37
  101.4 0.1 convert_reduce_fusion.1
  101.6 0.1 copy.37
  101.7 0.1 broadcast_in_dim.23
  101.8 18.4 %all_to_all.21 = bf16[8,256,256]{1,2,0:T(8,128)(2,1)S(1)} all-to-all(bf16[8,256,256]{1,2,0:T(8,128)(2,1)S(1)} %broadcast_in_dim.23), channel_id=1, replica_groups=mesh['rep'=4,'fs'=32,'tp'=8] {'tp'}, dimensions={0} | all-to-all | bytes 2097152 | tf_op jit(solution)/shard_map/all_to_all | solution.py:22
  120.2 0.3 multiply_reduce_fusion
  120.5 0.3 fusion.31
  120.8 128.9 %all-gather.2.cloned.1.call-done = bf16[2048,1056]{1,0:T(8,128)(2,1)} async-done(((bf16[64,1056]{1,0:T(8,128)(2,1)}), bf16[2048,1056]{1,0:T(8,128)(2,1)}) %all-gather.2.cloned.1.call-update) | async-done | bytes 4325392 | tf_op jit(solution)/shard_map/all_gather | solution.py:44
  249.7 2.2 fusion.37
  251.9 5.2 %convolution_convert_fusion = bf16[256,2048]{1,0:T(8,128)(2,1)S(1)} fusion(bf16[2048,1056]{1,0:T(8,128)(2,1)} %all-gather.2.cloned.1.call-done, bf16[256,2048]{0,1:T(8,128)(2,1)} %copy-done.3, f32[256,352]{0,1:T(8,128)S(1)} %fusion.37, f32[352]{0:T(512)S(1)} %copy-done.17), kind=kOutput, calls=%fused_computation.36 | convolution fusion | flops 739352576 | bytes 5604736 | tf_op jit(solution)/shard_map/dot_general | solution.py:131
  257.1 0.1 copy.47
  257.2 38.9 %all_to_all.22 = bf16[8,256,256]{2,1,0:T(8,128)(2,1)S(1)} all-to-all(bf16[8,256,256]{2,1,0:T(8,128)(2,1)S(1)} %bitcast.201), channel_id=1, replica_groups=mesh['rep'=4,'fs'=32,'tp'=8] {'tp'}, dimensions={0} | all-to-all | bytes 2097152 | tf_op jit(solution)/shard_map/all_to_all | solution.py:37
  296.1 0.1 convert_reduce_fusion
  296.2 0.7 fusion.59
  (60 shorter events, 0.3 us)
Async XLA Ops:
  6.5 18.3 %copy-start.8 = (f32[64,352]{1,0:T(8,128)S(1)}, f32[64,352]{1,0:T(8,128)}, u32[]{:S(2)}) copy-start(f32[64,352]{1,0:T(8,128)} %param.30) | copy-start | bytes 270340
  6.5 18.3 %copy-start.9 = (f32[64,352]{1,0:T(8,128)S(1)}, f32[64,352]{1,0:T(8,128)}, u32[]{:S(2)}) copy-start(f32[64,352]{1,0:T(8,128)} %param.32) | copy-start | bytes 270340
  6.5 18.4 %copy-start.10 = (f32[64,352]{1,0:T(8,128)S(1)}, f32[64,352]{1,0:T(8,128)}, u32[]{:S(2)}) copy-start(f32[64,352]{1,0:T(8,128)} %param.34) | copy-start | bytes 270340
  6.5 19.2 %copy-start.4 = (bf16[1,256,256]{2,1,0:T(8,128)(2,1)S(1)}, bf16[1,256,256]{2,1,0:T(8,128)(2,1)}, u32[]{:S(2)}) copy-start(bf16[1,256,256]{2,1,0:T(8,128)(2,1)} %param.22) | copy-start | bytes 393220
  8.6 17.4 %copy-start = (bf16[1,256,256]{2,1,0:T(8,128)(2,1)S(1)}, bf16[1,256,256]{2,1,0:T(8,128)(2,1)}, u32[]{:S(2)}) copy-start(bf16[1,256,256]{2,1,0:T(8,128)(2,1)} %param.23) | copy-start | bytes 393220
  8.6 17.6 %copy-start.1 = (f32[1,256,256]{2,1,0:T(8,128)S(1)}, f32[1,256,256]{2,1,0:T(8,128)}, u32[]{:S(2)}) copy-start(f32[1,256,256]{2,1,0:T(8,128)} %param.24) | copy-start | bytes 786436
  8.6 17.6 %copy-start.12 = (f32[1,256,1]{1,2,0:T(1,128)S(1)}, f32[1,256,1]{1,2,0:T(1,128)}, u32[]{:S(2)}) copy-start(f32[1,256,1]{1,2,0:T(1,128)} %param.25) | copy-start | bytes 3076
  8.6 66.5 %all-to-all-start = ((bf16[32,64,256]{2,1,0:T(8,128)(2,1)}), bf16[32,64,256]{2,1,0:T(8,128)(2,1)S(1)}, u32[]{:S(2)}, u32[]{:S(2)}) async-start(bf16[32,64,256]{2,1,0:T(8,128)(2,1)} %broadcast_in_dim.21), calls=%async_computation | async-start | bytes 2097152 | tf_op jit(solution)/shard_map/all_to_all | solution.py:22
  24.8 224.9 %all-gather.2.cloned.1.call-start = ((), (), s32[]{:S(2)}) async-start(), calls=%async_computation.4 | async-start | bytes 4866048 | tf_op jit(solution)/shard_map/all_gather | solution.py:44
  39.4 4.0 %copy-start.2 = (f32[1,256,256]{2,1,0:T(8,128)S(1)}, f32[1,256,256]{2,1,0:T(8,128)}, u32[]{:S(2)}) copy-start(f32[1,256,256]{2,1,0:T(8,128)} %param.24) | copy-start | bytes 786436
  39.4 4.5 %copy-start.5 = (bf16[1,256,256]{2,1,0:T(8,128)(2,1)S(1)}, bf16[1,256,256]{2,1,0:T(8,128)(2,1)}, u32[]{:S(2)}) copy-start(bf16[1,256,256]{2,1,0:T(8,128)(2,1)} %param.21) | copy-start | bytes 393220
  39.4 4.5 %copy-start.6 = (f32[64,64]{1,0:T(8,128)S(1)}, f32[64,64]{1,0:T(8,128)}, u32[]{:S(2)}) copy-start(f32[64,64]{1,0:T(8,128)} %fusion.84) | copy-start | bytes 49156
  44.5 30.6 %copy-start.13 = (f32[256]{0:T(256)S(1)}, f32[256]{0:T(256)}, u32[]{:S(2)}) copy-start(f32[256]{0:T(256)} %param.26) | copy-start | bytes 3076
  75.7 25.8 %copy-start.7 = (bf16[1,256,256]{2,1,0:T(8,128)(2,1)S(1)}, bf16[1,256,256]{2,1,0:T(8,128)(2,1)}, u32[]{:S(2)}) copy-start(bf16[1,256,256]{2,1,0:T(8,128)(2,1)} %param.20) | copy-start | bytes 393220
  75.7 25.8 %copy-start.14 = (f32[256]{0:T(256)S(1)}, f32[256]{0:T(256)}, u32[]{:S(2)}) copy-start(f32[256]{0:T(256)} %param.28) | copy-start | bytes 3076
  101.7 18.8 %copy-start.11 = (f32[2048]{0:T(1024)S(1)}, f32[2048]{0:T(1024)}, u32[]{:S(2)}) copy-start(f32[2048]{0:T(1024)} %param.29) | copy-start | bytes 24580
  120.2 129.6 %copy-start.16 = (f32[352]{0:T(512)S(1)}, f32[352]{0:T(512)}, u32[]{:S(2)}) copy-start(f32[352]{0:T(512)} %param.31) | copy-start | bytes 4228
  120.8 128.9 %copy-start.3 = (bf16[256,2048]{0,1:T(8,128)(2,1)}, bf16[256,2048]{0,1:T(8,128)(2,1)S(1)}, u32[]{:S(2)}) copy-start(bf16[256,2048]{0,1:T(8,128)(2,1)S(1)} %fusion.31) | copy-start | bytes 3145732
  120.8 131.1 %copy-start.17 = (f32[352]{0:T(512)S(1)}, f32[352]{0:T(512)}, u32[]{:S(2)}) copy-start(f32[352]{0:T(512)} %param.33) | copy-start | bytes 4228
  257.1 39.1 %copy-start.15 = (f32[256]{0:T(256)S(1)}, f32[256]{0:T(256)}, u32[]{:S(2)}) copy-start(f32[256]{0:T(256)} %param.35) | copy-start | bytes 3076
Sparse Core Ops, SparseCore 0:
  28.3 221.3 all-gather.1
where the time goes:
time: 305 us; the launch traced here: 304 us
  waiting for transfers between devices  156 us (51%)
  blocking collectives  83 us (27%)
  matrix products  22.8 us (7%)
  starting transfers between devices  16.3 us (5%)
  between operations  13.9 us (5%)
  local copies, waits for them, and re-layouts  5.95 us (2%)
  other arithmetic  5.79 us (2%)
    all_gather x1, waiting for transfers between devices, sent_together(): whole = lax.all_gather(both, axis, axis=dim, tiled=True)  129 us
    all_to_all x2, blocking collectives, summed_on_arrival(): lax.all_to_all(pieces, axis, split_axis=0, concat_axis=0, tiled=True)  64.6 us
    all_to_all x1, waiting for transfers between devices, sent_to_all(): lax.all_to_all(jnp.broadcast_to(x[None], (length, *x.shape)), axis, 0, 0,...  27 us
    all_to_all x1, blocking collectives, sent_to_all(): lax.all_to_all(jnp.broadcast_to(x[None], (length, *x.shape)), axis, 0, 0,...  18.4 us
    all_to_all x1, starting transfers between devices, sent_to_all(): lax.all_to_all(jnp.broadcast_to(x[None], (length, *x.shape)), axis, 0, 0,...  16.2 us
    dot_general x8, matrix products, advance(): carried = jnp.einsum('shcd,shde->shce', q_piece, memory, precision=highest)  7.87 us
  transfers between devices with their start and end apart: 2, of which 2 were waited for; matrix products, arithmetic and copies ran while one was open for 8% of the time, Pallas kernels for 0%

commit v1 on v0

v1 whole, which is shorter than its diff:
```python
import functools

import jax
import jax.numpy as jnp
from jax import lax
from jax.experimental import pallas as pl
from jax.experimental.pallas import tpu as pltpu
from jax.sharding import PartitionSpec as P

MESH = pl.DeviceIdType.MESH
F32, BF16 = jnp.float32, jnp.bfloat16
EPS = 1e-06

RELAY_Z = [(0, 1, 0), (0, -1, 0), (1, 2, 0), (-1, -2, 0), (2, 3, 0), (-2, -3, 0), (3, 4, 1), (-3, -4, 2)]
DIRECT_Z = [(0, 1, 0), (0, -1, 0), (0, 2, 0), (0, -2, 0), (0, 3, 0), (0, -3, 0), (0, 4, 1), (0, -4, 2)]
SKIP_Z = [(0, 1, 0), (0, -1, 0), (0, 2, 0), (0, -2, 0), (2, 3, 0), (-2, -3, 0), (2, 4, 1), (-2, -4, 2)]
RELAY_Y = [(0, 1, 0), (0, -1, 0), (1, 2, 1), (-1, -2, 2)]
DIRECT_Y = [(0, 1, 0), (0, -1, 0), (0, 2, 1), (0, -2, 2)]
OFFSETS = (0, 1, -1, 2, -2, 3, -3, 4)

STAGES = ((16, SKIP_Z, DIRECT_Y), (32, RELAY_Z, RELAY_Y), (16, RELAY_Z, RELAY_Y))
HALVES = 2
N_GATHER = 52
N_REDUCE = 7 * HALVES
N_SPREAD = 7 * HALVES
N_COPIES = 3 * N_GATHER + 2 * N_REDUCE + N_SPREAD

ORDER = (
    ("A0", "B0", "C0", "pre", "att0", "att1", "att2", "att3", "A1", "A2", "B1", "C1", "A9"),
    ("R0", "B2", "C2", "R1", "B3", "C3", "R2", "B4", "C4", "S0", "B5", "C5", "S1", "B6", "C6", "S2", "B9"),
    ("H0", "C9", "D0", "D1", "D2", "O0"),
)


def dot_rows(a, b):
    return lax.dot_general(a, b, (((1,), (1,)), ((), ())), preferred_element_type=F32)


def dot_plain(a, b):
    return lax.dot_general(a, b, (((1,), (0,)), ((), ())), preferred_element_type=F32)


def kernel(*refs):
    inputs, rest = refs[:16], refs[16:]
    upd_ref, tot_ref = rest[:2]
    staged, rest = rest[2:18], rest[18:]
    (
        wa, wb, wc, lc, mc, nrm, hid, uall, nin,
        px, pr, own, sa, sb, sc, ra, rb, rc,
        load_sem, send_sem, recv_sem,
    ) = rest
    res, q, k, v, lod, sur, hg, ow, ocs, png, gw, gcs, uw, ucs, dw, dcs = staged
    rep, fs, tp = (lax.axis_index(n) for n in ("rep", "fs", "tp"))
    zl, y = lax.div(fs, 4), lax.rem(fs, 4)
    x, c = lax.div(tp, 2), lax.rem(tp, 2)
    z = rep * 8 + zl
    sgn = 1 - 2 * c

    def at(dz=0, dy=0):
        zz = lax.rem(z + dz + 32, 32)
        return (lax.div(zz, 8), lax.rem(zz, 8) * 4 + lax.rem(y + dy + 4, 4), tp)

    def at_x(dx):
        return (rep, fs, 2 * lax.rem(x + dx + 4, 4) + c)

    partner = (rep, fs, 2 * x + 1 - c)

    class Copy:
        def __init__(self, i):
            self.i, self.sent, self.got = i, None, False

        def start(self, src, dst, to):
            self.sent = pltpu.make_async_remote_copy(
                src_ref=src, dst_ref=dst, send_sem=send_sem.at[self.i], recv_sem=recv_sem.at[self.i],
                device_id=to, device_id_type=MESH)
            self.sent.start()

        def wait(self, dst, to):
            if not self.got:
                self.got = True
                pltpu.make_async_remote_copy(
                    src_ref=dst, dst_ref=dst, send_sem=send_sem.at[self.i], recv_sem=recv_sem.at[self.i],
                    device_id=to, device_id_type=MESH).wait_recv()

    copies = [Copy(i) for i in range(N_COPIES)]
    free = iter(copies)

    barrier = pltpu.get_barrier_semaphore()
    peers = []
    dzs = sorted({child - parent for _, tree, _ in STAGES for parent, child, _ in tree})
    dys = sorted({child - parent for _, _, tree in STAGES for parent, child, _ in tree} - {-2})
    peers += [at(dz=d) for d in dzs] + [at(dy=d) for d in dys] + [at_x(1), at_x(-1), partner]
    for peer in peers:
        pl.semaphore_signal(barrier, inc=1, device_id=peer, device_id_type=MESH)

    loads = [pltpu.make_async_copy(inputs[i], staged[i], load_sem.at[i]) for i in range(16)]
    for i in (7, 10, 12, 14, 4, 5, 1, 2, 3, 6, 0, 8, 9, 11, 13, 15):
        loads[i].start()
    for i in (7, 10, 12, 14):
        loads[i].wait()
    wa[zl, y] = ow[...].astype(BF16)
    zpad = jnp.zeros((64, 32), BF16)
    wb[zl, y, :, 0:352] = gw[...].astype(BF16)
    wb[zl, y, :, 352:384] = zpad
    wb[zl, y, :, 384:736] = uw[...].astype(BF16)
    wb[zl, y, :, 736:768] = zpad
    wc[zl, y, :, 0:352] = dw[...].astype(BF16)
    wc[zl, y, :, 352:384] = zpad
    pl.semaphore_wait(barrier, len(peers))

    def stage_steps(buf, p, ztree, ytree):
        cp = {}

        def plane(d):
            return lax.rem(zl - d + 8, 8)

        def q_slice(dz, dy, part):
            zz, yy = plane(dz), lax.rem(y - dy + 4, 4)
            return zz, yy

        def q_ref(dz, dy, zpart, ypart):
            rows = 64 - p
            cut = 16 * (rows // 32) if rows > 16 else 0
            lo, hi = p, 64
            for part in (zpart, ypart):
                if part == 1:
                    hi = p + cut
                if part == 2:
                    lo = p + cut
            return buf.at[plane(dz), lax.rem(y - dy + 4, 4), lo:hi]

        def p_ref(dy, part):
            lo, hi = (0, p)
            if p > 16:
                if part == 1:
                    hi = p // 2
                if part == 2:
                    lo = p // 2
            return buf.at[zl, lax.rem(y - dy + 4, 4), lo:hi]

        def b_ref(dz, part):
            lo, hi = (0, 4) if part == 0 else ((0, 2) if part == 1 else (2, 4))
            return buf.at[plane(dz), lo:hi, 0:p]

        def p_skip(part):
            return p <= 16 and part == 2

        table = {}
        for parent, child, part in ytree:
            if p and not p_skip(part):
                table["py", child] = (parent, part)
        for parent, child, part in ztree:
            if p:
                table["pz", child] = (parent, part)
            table["qz", child] = (parent, part)
        for d in OFFSETS:
            for parent, child, part in ytree:
                table["qy", d, child] = (parent, part)
        for key in table:
            cp[key] = next(free)

        def refs(key, back):
            parent, part = table[key]
            d = parent if back else key[-1]
            step = key[-1] - parent
            if key[0] == "py":
                return p_ref(d, part), at(dy=step)
            if key[0] == "pz":
                return b_ref(d, part), at(dz=step)
            if key[0] == "qz":
                return q_ref(d, 0, part, 0), at(dz=step)
            return q_ref(key[1], d, 0, part), at(dy=step)

        def send(key):
            if key not in table:
                return
            parent = table[key][0]
            if key[0] in ("py", "qz"):
                if parent:
                    wait(key[:-1] + (parent,))
            elif key[0] == "pz":
                if parent:
                    wait(("pz", parent))
                else:
                    for n in (1, -1, 2, -2):
                        wait(("py", n))
            else:
                if parent:
                    wait(key[:-1] + (parent,))
                elif key[1] == 4:
                    wait(("qz", 4))
                    wait(("qz", -4))
                elif key[1]:
                    wait(("qz", key[1]))
            src, to = refs(key, True)
            cp[key].start(src, src, to)

        def wait(key):
            if key in table:
                dst, to = refs(key, False)
                cp[key].wait(dst, to)

        depth = {0: 0}
        for parent, child, _ in ztree:
            depth[child] = depth[parent] + 1
        last = max(depth.values())
        steps = []

        def add(r, key):
            while len(steps) <= r:
                steps.append([])
            steps[r].append(key)

        for key in [("py", 1), ("py", -1)]:
            add(0, key)
        ydepth = {0: 0}
        for parent, child, _ in ytree:
            ydepth[child] = ydepth[parent] + 1
        for key in [("py", 2), ("py", -2)]:
            add(ydepth[2] - 1, key)
        for parent, child, _ in ztree:
            add(depth[child] - 1, ("qz", child))
            add(depth[child] - 1 + ydepth[2], ("pz", child))
        for d in OFFSETS:
            for child in (1, -1):
                add(depth[d], ("qy", d, child))
            for child in (2, -2):
                add(depth[d] + ydepth[2] - 1, ("qy", d, child))

        def run(r):
            if r < len(steps):
                for key in steps[r]:
                    send(key)
            if r == 9:
                for key in table:
                    wait(key)

        return run

    stage = {
        "A": stage_steps(wa, *STAGES[0]),
        "B": stage_steps(wb, *STAGES[1]),
        "C": stage_steps(wc, *STAGES[2]),
    }

    def pre():
        for i in (4, 5, 1, 2, 3, 6, 0, 8, 9, 11, 13, 15):
            loads[i].wait()
        u = lod[...]
        ls = -(jnp.maximum(-u, 0.0) + jnp.log1p(jnp.exp(-jnp.abs(u)))) * (1.0 / 16.0)
        row = lax.broadcasted_iota(jnp.int32, (256, 256), 0)
        col = lax.broadcasted_iota(jnp.int32, (256, 256), 1)
        tri = jnp.where(col <= row, 1.0, 0.0).astype(BF16)
        hi = ls.astype(BF16)
        r1 = ls - hi.astype(F32)
        mid = r1.astype(BF16)
        lo = (r1 - mid.astype(F32)).astype(BF16)
        total = dot_plain(tri, hi) + (dot_plain(tri, mid) + dot_plain(tri, lo))
        srow = jnp.broadcast_to(sur[...], (256, 256))
        upto = jnp.sum(jnp.where(col <= row, srow, 0.0), axis=1, keepdims=True)
        before = jnp.sum(jnp.where(col < row, srow, 0.0), axis=1, keepdims=True)
        lc[...] = total + upto
        mc[...] = (total - ls) + before

    def attend(i):
        a, b = 64 * i, 64 * i + 64
        li, mi = lc[a:b], mc[a:b]
        qi, ki = q[a:b].astype(F32), k[a:b].astype(F32)
        mid = lc[a + 31 : a + 32]
        sf = dot_rows((qi * jnp.exp(li - mid)).astype(BF16), (ki * jnp.exp(mid - li)).astype(BF16))
        sb_ = dot_rows((qi * jnp.exp(mid - mi)).astype(BF16), (ki * jnp.exp(mi - mid)).astype(BF16))
        row = lax.broadcasted_iota(jnp.int32, (64, 64), 0)
        col = lax.broadcasted_iota(jnp.int32, (64, 64), 1)
        s = jnp.where(col <= row, sf, 0.0) + jnp.where(col >= row, sb_, 0.0)
        o = dot_plain(s.astype(BF16), v[a:b])
        if i > 0:
            edge = lc[a - 1 : a]
            kf = (k[0:a].astype(F32) * jnp.exp(edge - lc[0:a])).astype(BF16)
            s = dot_rows((qi * jnp.exp(li - edge)).astype(BF16), kf)
            o += dot_plain(s.astype(BF16), v[0:a])
        if i < 3:
            edge = lc[b - 1 : b]
            kb = (k[b:256].astype(F32) * jnp.exp(mc[b:256] - edge)).astype(BF16)
            s = dot_rows((qi * jnp.exp(edge - mi)).astype(BF16), kb)
            o += dot_plain(s.astype(BF16), v[b:256])
        o = o * (1.0 / 16.0)
        ms = jnp.mean(o * o, axis=1, keepdims=True)
        nrm[a:b] = (o * lax.rsqrt(ms + EPS) * hg[...]).astype(BF16)

    def ring_x(r, s):
        return lax.rem(x + (2, 4 - s, 4 + s, 0)[r], 4)

    T = 256 // HALVES

    def reducer(idx, lhs, weights):
        cps = [[next(free) for _ in range(7)] for _ in range(HALVES)]

        def w(j):
            full = weights[j]
            return full.reshape(256, full.shape[-1])

        def rows(h):
            return slice(h * T, h * T + T)

        def first(h):
            cp = cps[h]
            for r in range(4):
                px[idx, h, r] = dot_rows(lhs[rows(h)], w(2 * ring_x(r, -sgn) + 1 - c)).astype(BF16)
            for r in range(4):
                own[h, r] = dot_rows(lhs[rows(h)], w(2 * ring_x(r, sgn) + c))
                cp[r].start(px.at[idx, h, r], pr.at[idx, h, r], partner)

        def second(h):
            cp = cps[h]
            for r, buf in ((0, sa), (1, sb)):
                cp[r].wait(pr.at[idx, h, r], partner)
                buf[idx, h] = (own[h, r] + pr[idx, h, r].astype(F32)).astype(BF16)
            for r in (2, 3):
                cp[r].wait(pr.at[idx, h, r], partner)
                own[h, r] = own[h, r] + pr[idx, h, r].astype(F32)
            cp[4].start(sa.at[idx, h], ra.at[idx, h], at_x(sgn))
            cp[5].start(sb.at[idx, h], rb.at[idx, h], at_x(-sgn))

        def third(h):
            cp = cps[h]
            cp[4].wait(ra.at[idx, h], at_x(sgn))
            sc[idx, h] = (own[h, 2] + ra[idx, h].astype(F32)).astype(BF16)
            cp[6].start(sc.at[idx, h], rc.at[idx, h], at_x(sgn))

        def total(h):
            cp = cps[h]
            cp[5].wait(rb.at[idx, h], at_x(-sgn))
            cp[6].wait(rc.at[idx, h], at_x(sgn))
            return own[h, 3] + rb[idx, h].astype(F32) + rc[idx, h].astype(F32)

        return first, second, third, total, rows

    mix = reducer(0, nrm, wa)
    down = reducer(1, hid, wc)

    cps = [[next(free) for _ in range(7)] for _ in range(HALVES)]

    def u_ref(h, j):
        return uall.at[j, h * T : h * T + T]

    def spread_own(h):
        cp = cps[h]
        total = mix[3](h)
        sl = mix[4](h)
        u = (res[sl].astype(F32) + ocs[...] * total).astype(BF16)
        uall[tp, sl] = u
        upd_ref[sl] = u
        cp[0].start(u_ref(h, tp), u_ref(h, tp), at_x(sgn))
        cp[1].start(u_ref(h, tp), u_ref(h, tp), at_x(-sgn))
        cp[3].start(u_ref(h, tp), u_ref(h, tp), partner)

    def spread_on(h):
        cp = cps[h]
        j = 2 * ring_x(1, sgn) + c
        cp[0].wait(u_ref(h, j), at_x(sgn))
        cp[2].start(u_ref(h, j), u_ref(h, j), at_x(sgn))
        cp[4].start(u_ref(h, j), u_ref(h, j), partner)
        j = 2 * ring_x(2, sgn) + c
        cp[1].wait(u_ref(h, j), at_x(-sgn))
        cp[5].start(u_ref(h, j), u_ref(h, j), partner)

    def spread_end(h):
        cp = cps[h]
        j = 2 * ring_x(0, sgn) + c
        cp[2].wait(u_ref(h, j), at_x(sgn))
        cp[6].start(u_ref(h, j), u_ref(h, j), partner)

    def normalise(h):
        cp = cps[h]
        for n, r in ((3, 3), (4, 1), (5, 2), (6, 0)):
            cp[n].wait(u_ref(h, 2 * ring_x(r, -sgn) + 1 - c), partner)
        sl = mix[4](h)
        ssq = jnp.zeros((T, 1), F32)
        for j in range(8):
            u = uall[j, sl].astype(F32)
            ssq += jnp.sum(u * u, axis=1, keepdims=True)
        factor = lax.rsqrt(ssq * (1.0 / 2048.0) + EPS)
        for j in range(8):
            u = uall[j, sl].astype(F32)
            nin[sl, 256 * j : 256 * j + 256] = (u * factor * png[:, 256 * j : 256 * j + 256]).astype(BF16)

    def hidden(h):
        normalise(h)
        sl = mix[4](h)
        gu = dot_plain(nin[sl], wb[...].reshape(2048, 768))
        g = gu[:, 0:352] * gcs[...]
        up = gu[:, 384:736] * ucs[...]
        hid[sl, 0:352] = (g / (1.0 + jnp.exp(-g)) * up).astype(BF16)
        hid[sl, 352:384] = jnp.zeros((T, 32), BF16)

    def out(h):
        sl = mix[4](h)
        tot_ref[sl] = dcs[...] * down[3](h)

    per_half = {
        "R0": mix[0], "R1": mix[1], "R2": mix[2], "S0": spread_own, "S1": spread_on, "S2": spread_end,
        "H0": hidden, "D0": down[0], "D1": down[1], "D2": down[2], "O0": out,
    }

    for token in sum(ORDER, ()):
        if token[0] in stage:
            stage[token[0]](int(token[1:]))
        elif token == "pre":
            pre()
        elif token[:3] == "att":
            attend(int(token[3:]))
        elif token[2:] == "":
            for h in range(HALVES):
                per_half[token](h)
        else:
            per_half[token[:2]](int(token[2:]))

    for cp in copies:
        if cp.sent is not None:
            cp.sent.wait_send()


def body(res, q, k, v, lod, sur, hg, ow, ocs, png, gw, gcs, uw, ucs, dw, dcs):
    rows = 256
    flat = (
        res.reshape(rows, -1), q.reshape(rows, -1), k.reshape(rows, -1), v.reshape(rows, -1),
        lod.reshape(rows, -1), sur.reshape(1, rows), hg.reshape(1, -1), ow, ocs.reshape(1, -1),
        png.reshape(1, -1), gw, gcs, uw, ucs, dw, dcs.reshape(1, -1),
    )
    H, T = HALVES, 256 // HALVES
    vm = pltpu.VMEM
    upd, total = pl.pallas_call(
        kernel,
        name="layer",
        out_shape=(jax.ShapeDtypeStruct((rows, 256), BF16), jax.ShapeDtypeStruct((rows, 256), F32)),
        in_specs=[pl.BlockSpec(memory_space=pl.ANY)] * 16,
        out_specs=[pl.BlockSpec(memory_space=pltpu.VMEM)] * 2,
        scratch_shapes=[vm(a.shape, a.dtype) for a in flat] + [
            vm((8, 4, 64, 256), BF16), vm((8, 4, 64, 768), BF16), vm((8, 4, 64, 384), BF16),
            vm((256, 256), F32), vm((256, 256), F32), vm((256, 256), BF16), vm((256, 384), BF16),
            vm((8, 256, 256), BF16), vm((256, 2048), BF16),
            vm((2, H, 4, T, 256), BF16), vm((2, H, 4, T, 256), BF16), vm((H, 4, T, 256), F32),
            vm((2, H, T, 256), BF16), vm((2, H, T, 256), BF16), vm((2, H, T, 256), BF16),
            vm((2, H, T, 256), BF16), vm((2, H, T, 256), BF16), vm((2, H, T, 256), BF16),
            pltpu.SemaphoreType.DMA((16,)),
            pltpu.SemaphoreType.DMA((N_COPIES,)), pltpu.SemaphoreType.DMA((N_COPIES,)),
        ],
        compiler_params=pltpu.CompilerParams(
            collective_id=0, has_side_effects=True, vmem_limit_bytes=56 * 2**20),
    )(*flat)
    result = (upd.astype(F32) + total).astype(BF16)
    return result.reshape(1, rows, 256)


def solution(mesh):
    seq = P(("rep", "fs"), None, "tp")
    return jax.shard_map(
        body,
        mesh=mesh,
        in_specs=(
            seq, seq, seq, seq, seq, seq, P(), P("fs", "tp"), P("tp"), P(),
            P("fs", "tp"), P("tp"), P("fs", "tp"), P("tp"), P("fs", "tp"), P("tp"),
        ),
        out_specs=seq,
        check_vma=False,
    )
```

time: 305 us -> 79.6 us (0.26)
  waiting for transfers between devices: 156 us -> 0 us
  blocking collectives: 83 us -> 0 us
  Pallas kernels: 0 us -> 77.8 us
  matrix products: 22.8 us -> 0 us
  starting transfers between devices: 16.3 us -> 0 us
  between operations: 13.9 us -> 0.01 us
  local copies, waits for them, and re-layouts: 5.95 us -> 0 us
  other arithmetic: 5.79 us -> 1.67 us
    all_gather x1 -> x0, waiting for transfers between devices: 129 us -> none  [sent_together(): whole = lax.all_gather(both, axis, axis=dim, tiled=True)]
    all_to_all x3 -> x0, blocking collectives: 83 us -> none  [the longest x2 64.6 us: summed_on_arrival(): lax.all_to_all(pieces, axis, split_axis=0, concat_axis=0, tiled=True)]
    pallas_call x0 -> x1, Pallas kernels: none -> 77.8 us  [body(): pl.pallas_call(kernel, name='layer', out_shape=(jax.ShapeDtypeStruct((row...]
    all_to_all x1 -> x0, waiting for transfers between devices: 27 us -> none  [sent_to_all(): lax.all_to_all(jnp.broadcast_to(x[None], (length, *x.shape)), axis, 0, 0,...]
    dot_general x23 -> x0, matrix products: 22.8 us -> none  [the longest x8 7.87 us: advance(): carried = jnp.einsum('shcd,shde->shce', q_piece, memory, precision=highest)]
    all_to_all x1 -> x0, starting transfers between devices: 16.2 us -> none  [sent_to_all(): lax.all_to_all(jnp.broadcast_to(x[None], (length, *x.shape)), axis, 0, 0,...]
  transfers between devices with their start and end apart: 2 -> 0, of which waited for: 2 -> 0; matrix products, arithmetic and copies ran while one was open for 8% -> 0% of each run, Pallas kernels for 0% -> 0%
where the time goes in v1:
time: 79.6 us; the launch traced here: 79.5 us
  Pallas kernels  77.8 us (98%)
  other arithmetic  1.67 us (2%)
    pallas_call x1, Pallas kernels, body(): pl.pallas_call(kernel, name='layer', out_shape=(jax.ShapeDtypeStruct((row...  77.8 us
    reshape x1, other arithmetic, body(): return result.reshape(1, rows, 256)  1.67 us

profile of v1, /device:TPU:1, one launch (start us, length us, event | category | flops | bytes accessed | tf_op | source)
XLA Modules:
  0.0 79.5 jit_solution(5319610170554985747)
XLA Ops:
  0.0 77.8 %layer.1 = (bf16[256,256]{1,0:T(8,128)(2,1)}, f32[256,256]{1,0:T(8,128)}) custom-call(bf16[256,256]{1,0:T(8,128)(2,1)} %bitcast.13, bf16[256,256]{1,0:T(8,128)(2,1)} %bitcast.14, bf16[256,256]{1,0:T(8,128)(2,1)} %bitcast.15, bf16[256,256]{1,0:T(8,128)(2,1)} %bitcast.16, f32[256,256]{1,0:T(8,128)} %bitcast.12, f32[1,256]{1,0:T(1,128)} %bitcast.18, ...), custom_call_target="tpu_custom_call" | custom-call | tf_op jit(solution)/shard_map/layer/pallas_call | solution.py:432
  77.8 1.7 %fusion = bf16[1,256,256]{2,1,0:T(8,128)(2,1)} fusion(f32[256,256]{1,0:T(8,128)} %get-tuple-element.8, bf16[256,256]{1,0:T(8,128)(2,1)} %get-tuple-element.7), kind=kLoop, calls=%fused_computation.1 | loop fusion | flops 196608 | bytes 524288 | tf_op jit(solution)/shard_map/reshape | solution.py:452

commit v2 on v1

--- a/solution.py
+++ b/solution.py
@@ -18,7 +18,7 @@
 DIRECT_Y = [(0, 1, 0), (0, -1, 0), (0, 2, 1), (0, -2, 2)]
 OFFSETS = (0, 1, -1, 2, -2, 3, -3, 4)
 
-STAGES = ((16, SKIP_Z, DIRECT_Y), (32, RELAY_Z, RELAY_Y), (16, RELAY_Z, RELAY_Y))
+STAGES = ((32, SKIP_Z, DIRECT_Y), (16, RELAY_Z, RELAY_Y), (32, RELAY_Z, RELAY_Y))
 HALVES = 2
 N_GATHER = 52
 N_REDUCE = 7 * HALVES
@@ -26,8 +26,8 @@
 N_COPIES = 3 * N_GATHER + 2 * N_REDUCE + N_SPREAD
 
 ORDER = (
-    ("A0", "B0", "C0", "pre", "att0", "att1", "att2", "att3", "A1", "A2", "B1", "C1", "A9"),
-    ("R0", "B2", "C2", "R1", "B3", "C3", "R2", "B4", "C4", "S0", "B5", "C5", "S1", "B6", "C6", "S2", "B9"),
+    ("A0", "B0", "C0", "pre", "att0", "att1", "att2", "att3", "A1", "B1", "A2", "B2", "C1", "A9"),
+    ("B3", "R0", "R1", "C2", "R2", "B4", "C3", "S0", "B5", "C4", "S1", "B6", "C5", "S2", "C6", "B9"),
     ("H0", "C9", "D0", "D1", "D2", "O0"),
 )
 
@@ -113,10 +113,6 @@
 
         def plane(d):
             return lax.rem(zl - d + 8, 8)
-
-        def q_slice(dz, dy, part):
-            zz, yy = plane(dz), lax.rem(y - dy + 4, 4)
-            return zz, yy
 
         def q_ref(dz, dy, zpart, ypart):
             rows = 64 - p
@@ -302,30 +298,48 @@
         def rows(h):
             return slice(h * T, h * T + T)
 
-        def first(h):
-            cp = cps[h]
-            for r in range(4):
-                px[idx, h, r] = dot_rows(lhs[rows(h)], w(2 * ring_x(r, -sgn) + 1 - c)).astype(BF16)
-            for r in range(4):
-                own[h, r] = dot_rows(lhs[rows(h)], w(2 * ring_x(r, sgn) + c))
-                cp[r].start(px.at[idx, h, r], pr.at[idx, h, r], partner)
-
-        def second(h):
-            cp = cps[h]
-            for r, buf in ((0, sa), (1, sb)):
-                cp[r].wait(pr.at[idx, h, r], partner)
-                buf[idx, h] = (own[h, r] + pr[idx, h, r].astype(F32)).astype(BF16)
-            for r in (2, 3):
-                cp[r].wait(pr.at[idx, h, r], partner)
-                own[h, r] = own[h, r] + pr[idx, h, r].astype(F32)
-            cp[4].start(sa.at[idx, h], ra.at[idx, h], at_x(sgn))
-            cp[5].start(sb.at[idx, h], rb.at[idx, h], at_x(-sgn))
-
-        def third(h):
-            cp = cps[h]
-            cp[4].wait(ra.at[idx, h], at_x(sgn))
-            sc[idx, h] = (own[h, 2] + ra[idx, h].astype(F32)).astype(BF16)
-            cp[6].start(sc.at[idx, h], rc.at[idx, h], at_x(sgn))
+        def across(h, r):
+            px[idx, h, r] = dot_rows(lhs[rows(h)], w(2 * ring_x(r, -sgn) + 1 - c)).astype(BF16)
+            cps[h][r].start(px.at[idx, h, r], pr.at[idx, h, r], partner)
+
+        def mine(h, r):
+            own[h, r] = dot_rows(lhs[rows(h)], w(2 * ring_x(r, sgn) + c))
+
+        def pair(h, r):
+            cps[h][r].wait(pr.at[idx, h, r], partner)
+            return own[h, r] + pr[idx, h, r].astype(F32)
+
+        def first():
+            for h in range(HALVES):
+                across(h, 0)
+            for h in range(HALVES):
+                mine(h, 0)
+                across(h, 1)
+            for h in range(HALVES):
+                sa[idx, h] = pair(h, 0).astype(BF16)
+                cps[h][4].start(sa.at[idx, h], ra.at[idx, h], at_x(sgn))
+                across(h, 2)
+
+        def second():
+            for h in range(HALVES):
+                mine(h, 1)
+                sb[idx, h] = pair(h, 1).astype(BF16)
+                cps[h][5].start(sb.at[idx, h], rb.at[idx, h], at_x(-sgn))
+            for h in range(HALVES):
+                mine(h, 2)
+                across(h, 3)
+            for h in range(HALVES):
+                own[h, 2] = pair(h, 2)
+
+        def third():
+            for h in range(HALVES):
+                cps[h][4].wait(ra.at[idx, h], at_x(sgn))
+                sc[idx, h] = (own[h, 2] + ra[idx, h].astype(F32)).astype(BF16)
+                cps[h][6].start(sc.at[idx, h], rc.at[idx, h], at_x(sgn))
+            for h in range(HALVES):
+                mine(h, 3)
+            for h in range(HALVES):
+                own[h, 3] = pair(h, 3)
 
         def total(h):
             cp = cps[h]
@@ -397,9 +411,10 @@
         sl = mix[4](h)
         tot_ref[sl] = dcs[...] * down[3](h)
 
+    whole = {"R0": mix[0], "R1": mix[1], "R2": mix[2], "D0": down[0], "D1": down[1], "D2": down[2]}
     per_half = {
-        "R0": mix[0], "R1": mix[1], "R2": mix[2], "S0": spread_own, "S1": spread_on, "S2": spread_end,
-        "H0": hidden, "D0": down[0], "D1": down[1], "D2": down[2], "O0": out,
+        "S0": spread_own, "S1": spread_on, "S2": spread_end,
+        "H0": hidden, "O0": out,
     }
 
     for token in sum(ORDER, ()):
@@ -409,6 +424,8 @@
             pre()
         elif token[:3] == "att":
             attend(int(token[3:]))
+        elif token in whole:
+            whole[token]()
         elif token[2:] == "":
             for h in range(HALVES):
                 per_half[token](h)
@@ -432,7 +449,7 @@
     upd, total = pl.pallas_call(
         kernel,
         name="layer",
-        out_shape=(jax.ShapeDtypeStruct((rows, 256), BF16), jax.ShapeDtypeStruct((rows, 256), F32)),
+        out_shape=(pltpu.VMEM((rows, 256), BF16), pltpu.VMEM((rows, 256), F32)),
         in_specs=[pl.BlockSpec(memory_space=pl.ANY)] * 16,
         out_specs=[pl.BlockSpec(memory_space=pltpu.VMEM)] * 2,
         scratch_shapes=[vm(a.shape, a.dtype) for a in flat] + [

time: 79.6 us -> 76.4 us (0.960); the launches traced: 79.5 us -> 75.5 us
  Pallas kernels: 77.8 us -> 74.8 us
  other arithmetic: 1.67 us -> 0.68 us
    pallas_call x1, Pallas kernels: 77.8 us -> 74.8 us  [body(): pl.pallas_call(kernel, name='layer', out_shape=(pltpu.VMEM((rows, 256), B...]
    reshape x1, other arithmetic: 1.67 us -> 0.68 us  [body(): return result.reshape(1, rows, 256)]
where the time goes in v2:
time: 76.4 us; the launch traced here: 75.5 us
  Pallas kernels  74.8 us (98%)
    pallas_call x1, Pallas kernels, body(): pl.pallas_call(kernel, name='layer', out_shape=(pltpu.VMEM((rows, 256), B...  74.8 us

profile of v2, /device:TPU:1, one launch (start us, length us, event | category | flops | bytes accessed | tf_op | source)
XLA Modules:
  0.0 75.5 jit_solution(5533176965859334110)
XLA Ops:
  0.0 74.8 %layer.1 = (bf16[256,256]{1,0:T(8,128)(2,1)S(1)}, f32[256,256]{1,0:T(8,128)S(1)}) custom-call(bf16[256,256]{1,0:T(8,128)(2,1)} %bitcast.13, bf16[256,256]{1,0:T(8,128)(2,1)} %bitcast.14, bf16[256,256]{1,0:T(8,128)(2,1)} %bitcast.15, bf16[256,256]{1,0:T(8,128)(2,1)} %bitcast.16, f32[256,256]{1,0:T(8,128)} %bitcast.12, f32[1,256]{1,0:T(1,128)} %bitcast.18, ...), custom_call_target="tpu_custom_call" | custom-call | tf_op jit(solution)/shard_map/layer/pallas_call | solution.py:449
  74.8 0.7 fusion
